TPU v7x, 32 devices: a whole 2x2x4 slice. The times are simulated.
32 devices in a mesh: sp: 8 (over z, x), tp: 4 (over y, core).
Axes of the slice: x: 2, y: 2, z: 4, core: 2. Of those that a mesh axis runs over, the one named last changes fastest.
Arguments:
- queries: bfloat16 [4096, 2048], P('sp', 'tp'), may hold values from -90 to 90, as said below
- key_rows: bfloat16 [4096, 512], P('sp', 'tp'), may hold values from -6 to 6
- value_rows: bfloat16 [4096, 512], P('sp', 'tp'), may hold values from -6 to 6
- sink_logits: float32 [16], P('tp'), may hold values from 2 to 7
- residual: bfloat16 [4096, 2048], P('sp'), may hold values from -6 to 6
- norm_gain: float32 [2048], replicated, may hold values from 0.1 to 1.9
- out_weight: bfloat16 [2048, 2048], P('tp'), may hold values from -1.5 to 1.5
- gate_weight: bfloat16 [2048, 5632], P('sp', 'tp'), may hold values from -0.125 to 0.125
- up_weight: bfloat16 [2048, 5632], P('sp', 'tp'), may hold values from -0.125 to 0.125
- down_weight: bfloat16 [5632, 2048], P('tp', 'sp'), may hold values from -0.078125 to 0.078125
Outputs:
- mixed: bfloat16 [4096, 2048], P(('sp', 'tp'))
Inputs may be any that keep to these rules, and one draw needn't show every extreme that they name: queries are mostly of order one; some rows may be much larger.
All inputs are finite; a program needn't handle non-finite values.
Results may differ from a plain program's by a relative error of at most 0.012.
Values may be sent and summed in bfloat16 or wider, within the bound.
A program may use at most 128 MiB of HBM per device.

v0:
```python
import jax
import jax.numpy as jnp
from jax import lax
from jax.sharding import PartitionSpec as P

DH = 128
WIN = 128


EPSILON = 1e-06
MASKED = -1e30


def with_halo(cells, sides, width):
    for axis, dim in sides:
        count = lax.axis_size(axis)
        ends = count - 1
        head = lax.slice_in_dim(cells, 0, width, axis=dim)
        tail = lax.slice_in_dim(cells, cells.shape[dim] - width, cells.shape[dim], axis=dim)
        cells = jnp.concatenate(
            [
                lax.ppermute(tail, axis, [(i, (i + 1) % count) for i in range(ends)]),
                cells,
                lax.ppermute(head, axis, [((i + 1) % count, i) for i in range(ends)]),
            ],
            axis=dim,
        )
    return cells


def attend_block(query_blk, key_blk, value_blk, sink_logits, query_pos, key_pos, seq_len):
    kv_heads = key_blk.shape[1] // DH
    group_size = query_blk.shape[1] // key_blk.shape[1]
    query_four = query_blk.reshape(query_blk.shape[0], kv_heads, group_size, DH)
    key_three = key_blk.reshape(key_blk.shape[0], kv_heads, DH)
    value_three = value_blk.reshape(value_blk.shape[0], kv_heads, DH)
    scores = jnp.einsum(
        "qhgd,khd->hgqk", query_four, key_three, preferred_element_type=jnp.float32
    ) * DH ** (-0.5)
    allowed = (
        (jnp.abs(key_pos[None, :] - query_pos[:, None]) <= WIN)
        & (key_pos[None, :] >= 0)
        & (key_pos[None, :] < seq_len)
    )
    scores = jnp.where(allowed[None, None], scores, MASKED)
    sink_col = sink_logits.reshape(kv_heads, group_size)[:, :, None]
    highest = jnp.maximum(jnp.max(scores, axis=-1), sink_col)
    weights_exp = jnp.exp(scores - highest[..., None])
    denominator = jnp.sum(weights_exp, axis=-1) + jnp.exp(sink_col - highest)
    probabilities = (weights_exp / denominator[..., None]).astype(jnp.bfloat16)
    heads_out = jnp.einsum(
        "hgqk,khd->qhgd", probabilities, value_three, preferred_element_type=jnp.float32
    )
    return heads_out.astype(jnp.bfloat16).reshape(query_blk.shape[0], kv_heads * group_size * DH)


def rms_scale(rows_wide, norm_gain):
    mean_square = jnp.mean(rows_wide * rows_wide, axis=-1, keepdims=True)
    return (rows_wide * lax.rsqrt(mean_square + EPSILON) * norm_gain).astype(jnp.bfloat16)


def fetch_down(down_weight):
    return lax.all_gather(down_weight, "sp", axis=1, tiled=True)


def shards(
    queries,
    key_rows,
    value_rows,
    sink_logits,
    residual,
    norm_gain,
    out_weight,
    gate_weight,
    up_weight,
    down_weight,
):
    tok_local = queries.shape[0]
    block_len = 2 * WIN
    share_rows = tok_local // lax.axis_size("tp")
    seq_len = tok_local * lax.axis_size("sp")
    device_offset = lax.axis_index("sp") * tok_local
    kv_pair = jnp.stack([key_rows, value_rows])
    kv_ext = with_halo(kv_pair, (("sp", 1),), WIN)

    def one_block(block_index):
        block_first = block_index * block_len
        query_blk = lax.dynamic_slice_in_dim(queries, block_first, block_len, 0)
        key_blk = lax.dynamic_slice_in_dim(kv_ext[0], block_first, block_len + 2 * WIN, 0)
        value_blk = lax.dynamic_slice_in_dim(kv_ext[1], block_first, block_len + 2 * WIN, 0)
        query_pos = device_offset + block_first + jnp.arange(block_len, dtype=jnp.int32)
        key_pos = (
            device_offset + block_first - WIN + jnp.arange(block_len + 2 * WIN, dtype=jnp.int32)
        )
        return attend_block(query_blk, key_blk, value_blk, sink_logits, query_pos, key_pos, seq_len)

    blocks = lax.map(one_block, jnp.arange(tok_local // block_len, dtype=jnp.int32))
    attended = blocks.reshape(tok_local, queries.shape[1])
    own_first = lax.axis_index("tp") * share_rows
    attn_full = lax.psum(
        jnp.dot(attended, out_weight, preferred_element_type=jnp.float32).astype(jnp.bfloat16), "tp"
    ).astype(jnp.float32)
    middle_all = residual.astype(jnp.float32) + attn_full
    normed_all = rms_scale(middle_all, norm_gain)
    middle_own = lax.dynamic_slice_in_dim(middle_all, own_first, share_rows, 0)
    gate_sectioned = lax.all_gather(gate_weight, "sp", axis=0, tiled=True)
    up_sectioned = lax.all_gather(up_weight, "sp", axis=0, tiled=True)
    gate_acc = jnp.dot(normed_all, gate_sectioned, preferred_element_type=jnp.float32)
    up_acc = jnp.dot(normed_all, up_sectioned, preferred_element_type=jnp.float32)
    down_whole = fetch_down(down_weight)
    hidden = (jax.nn.silu(gate_acc) * up_acc).astype(jnp.bfloat16)
    ffn_share = lax.psum_scatter(
        jnp.dot(hidden, down_whole, preferred_element_type=jnp.float32).astype(jnp.bfloat16),
        "tp",
        scatter_dimension=0,
        tiled=True,
    ).astype(jnp.float32)
    return (middle_own + ffn_share).astype(jnp.bfloat16)


def solution(mesh):
    placed = (
        P("sp", "tp"),
        P("sp", "tp"),
        P("sp", "tp"),
        P("tp"),
        P("sp", None),
        P(),
        P("tp", None),
        P("sp", "tp"),
        P("sp", "tp"),
        P("tp", "sp"),
    )
    return jax.shard_map(
        shards, mesh=mesh, in_specs=placed, out_specs=P(("sp", "tp"), None), check_vma=False
    )
```

profile of v0, /device:TPU:1, one launch (start us, length us, event | category | flops | bytes accessed | tf_op | source)
XLA Modules:
  0.0 369.8 jit_solution(8707252518556242722)
XLA Ops:
  7.4 1.0 pad_maximum_fusion.2
  8.3 3.9 %collective-permute-start = (bf16[2,128,128]{2,1,0:T(8,128)(2,1)S(1)}, bf16[2,128,128]{2,1,0:T(8,128)(2,1)S(1)}, u32[]{:S(2)}, u32[]{:S(2)}) collective-permute-start(bf16[2,128,128]{2,1,0:T(8,128)(2,1)S(1)} %get-tuple-element.124), channel_id=1, source_target_pairs={{0,4},{4,8},{8,12},{12,16},{16,20},{20,24},{24,28},{1,5},{5,9},{9,... | collective-permute-start | bytes 196616 | tf_op jit(solution)/shard_map/ppermute | solution.py:22
  12.3 1.3 collective-permute-start.1
  13.6 3.7 collective-permute-done.1
  17.3 1.0 pad_maximum_fusion
  18.3 11.1 %while.12 = (s32[]{:T(128)}, bf16[2,256,512]{2,1,0:T(8,128)(2,1)}, bf16[2,768,128]{2,1,0:T(8,128)(2,1)S(1)}, s32[2]{0:T(128)S(1)}, s32[]{:T(128)}, /*index=5*/bf...) while((s32[]{:T(128)}, bf16[2,256,512]{2,1,0:T(8,128)(2,1)}, ...), condition=%wide.region_3.4_spmd, body=%wide.region_0.3_spmd.sunk | while | flops 273420544 | bytes 14467512 | solution.py:97
  18.3 0.6 dynamic_slice.42
  19.9 1.0 constant_dynamic-slice_fusion.2
  21.1 0.5 fusion.37
  21.6 0.3 fusion.38
  22.0 0.5 convolution_convert_fusion.4
  22.7 0.4 copy-done.2
  23.1 0.8 copy-done.3
  23.9 0.6 dynamic_slice.42
  25.5 1.0 constant_dynamic-slice_fusion.2
  26.6 0.5 fusion.37
  27.6 0.5 convolution_convert_fusion.4
  28.3 0.4 copy-done.2
  28.7 0.8 copy-done.3
  29.4 3.6 convolution_convert_fusion.1
  33.2 0.5 all-gather.4.cloned.1.call-update
  33.7 0.5 all-gather.6.cloned.1.call-update
  34.3 0.5 all-gather.8.cloned.1.call-update
  34.9 52.1 %all-reduce.2.cloned.1.call-done = bf16[512,2048]{1,0:T(8,128)(2,1)} async-done(((bf16[512,2048]{1,0:T(8,128)(2,1)}), bf16[512,2048]{1,0:T(8,128)(2,1)}) %all-reduce.2.cloned.1.call-update) | async-done | bytes 2097168 | tf_op jit(solution)/shard_map/psum | solution.py:100
  87.0 4.9 %convert_add_fusion = (f32[512,2048]{1,0:T(8,128)}, f32[512]{0:T(512)S(1)}) fusion(bf16[512,2048]{1,0:T(8,128)(2,1)} %all-reduce.2.cloned.1.call-done, bf16[512,2048]{1,0:T(8,128)(2,1)} %param.16), kind=kLoop, calls=%fused_computation.25 | loop fusion | flops 5242368 | bytes 8390656 | tf_op jit(solution)/shard_map/add | solution.py:103
  91.9 37.0 %all-gather.4.cloned.1.call-done = bf16[2048,1408]{1,0:T(8,128)(2,1)} async-done(((bf16[256,1408]{1,0:T(8,128)(2,1)}), bf16[2048,1408]{1,0:T(8,128)(2,1)}) %all-gather.4.cloned.1.call-update) | async-done | bytes 5767184 | tf_op jit(solution)/shard_map/all_gather | solution.py:106
  128.9 9.0 %fusion.14 = f32[512,1408]{1,0:T(8,128)} fusion(bf16[2048,1408]{1,0:T(8,128)(2,1)} %all-gather.4.cloned.1.call-done, f32[2048]{0:T(1024)S(1)} %copy-done.4, f32[512]{0:T(512)S(1)} %add_rsqrt_fusion, bf16[512,2048]{1,0:T(8,128)(2,1)} %all-reduce.2.cloned.1.call-done, bf16[512,2048]{1,0:T(8,128)(2,1)} %param.16), kind=kOutput, calls=%fused_computation.36 | convolution fusion | flops 2959081472 | bytes 12855296 | tf_op jit(solution)/shard_map/dot_general | solution.py:108
  137.9 83.3 %all-gather.6.cloned.1.call-done = bf16[2048,1408]{1,0:T(8,128)(2,1)} async-done(((bf16[256,1408]{1,0:T(8,128)(2,1)}), bf16[2048,1408]{1,0:T(8,128)(2,1)}) %all-gather.6.cloned.1.call-update) | async-done | bytes 5767184 | tf_op jit(solution)/shard_map/all_gather | solution.py:107
  221.2 93.9 %all-gather.8.cloned.1.call-done = bf16[1408,2048]{1,0:T(8,128)(2,1)} async-done(((bf16[1408,256]{1,0:T(8,128)(2,1)}), bf16[1408,2048]{1,0:T(8,128)(2,1)}) %all-gather.8.cloned.1.call-update) | async-done | bytes 5767184 | tf_op jit(solution)/shard_map/all_gather | solution.py:63
  315.1 14.6 %convolution_convert_fusion.2 = bf16[512,2048]{1,0:T(8,128)(2,1)} fusion(bf16[1408,2048]{1,0:T(8,128)(2,1)} %all-gather.8.cloned.1.call-done, bf16[2048,1408]{1,0:T(8,128)(2,1)} %all-gather.6.cloned.1.call-done, f32[512,1408]{1,0:T(8,128)} %fusion.14, f32[2048]{0:T(1024)S(1)} %copy-done.4, f32[512]{0:T(512)S(1)} %add_rsqrt_fusion, ...), kind=kOutput, calls=%fused_computation.29 | convolution fusion | flops 5917245440 | bytes 20719616 | tf_op jit(solution)/shard_map/dot_general | solution.py:113
  329.7 30.2 %reduce-scatter.2.cloned.1.call-done = bf16[128,2048]{1,0:T(8,128)(2,1)} async-done(((bf16[512,2048]{1,0:T(8,128)(2,1)}), bf16[128,2048]{1,0:T(8,128)(2,1)}) %reduce-scatter.2.cloned.1.call-update) | async-done | bytes 524304 | tf_op jit(solution)/shard_map/reduce_scatter | solution.py:112
  359.9 2.3 add_convert_fusion
  (44 shorter events, 2.1 us)
Async XLA Ops:
  7.4 22.1 %copy-start = (bf16[512,2048]{1,0:T(8,128)(2,1)S(1)}, bf16[512,2048]{1,0:T(8,128)(2,1)}, u32[]{:S(2)}) copy-start(bf16[512,2048]{1,0:T(8,128)(2,1)} %param.18) | copy-start | bytes 6291460
  7.4 79.7 %all-reduce.2.cloned.1.call-start = ((), (), s32[]{:S(2)}) async-start(), calls=%async_computation.1 | async-start | bytes 4194304 | tf_op jit(solution)/shard_map/psum | solution.py:100
  8.3 5.3 %collective-permute-start = (bf16[2,128,128]{2,1,0:T(8,128)(2,1)S(1)}, bf16[2,128,128]{2,1,0:T(8,128)(2,1)S(1)}, u32[]{:S(2)}, u32[]{:S(2)}) collective-permute-start(bf16[2,128,128]{2,1,0:T(8,128)(2,1)S(1)} %get-tuple-element.124), channel_id=1, source_target_pairs={{0,4},{4,8},{8,12},{12,16},{16,20},{20,24},{24,28},{1,5},{5,9},{9,... | collective-permute-start | bytes 196616 | tf_op jit(solution)/shard_map/ppermute | solution.py:22
  12.3 5.0 %collective-permute-start.1 = (bf16[2,128,128]{2,1,0:T(8,128)(2,1)S(1)}, bf16[2,128,128]{2,1,0:T(8,128)(2,1)S(1)}, u32[]{:S(2)}, u32[]{:S(2)}) collective-permute-start(bf16[2,128,128]{2,1,0:T(8,128)(2,1)S(1)} %get-tuple-element.125), channel_id=1, source_target_pairs={{4,0},{8,4},{12,8},{16,12},{20,16},{24,20},{28,24},{5,1},{9,5},{13... | collective-permute-start | bytes 196616 | tf_op jit(solution)/shard_map/ppermute | solution.py:24
  18.3 3.2 copy-start.1
  22.0 1.0 copy-start.2
  23.1 0.8 copy-start.3
  23.9 3.2 copy-start.1
  27.6 1.0 copy-start.2
  28.6 0.8 copy-start.3
  33.1 95.8 %all-gather.4.cloned.1.call-start = ((), (), s32[]{:S(2)}) async-start(), calls=%async_computation.2 | async-start | bytes 6488064 | tf_op jit(solution)/shard_map/all_gather | solution.py:106
  33.7 187.5 %all-gather.6.cloned.1.call-start = ((), (), s32[]{:S(2)}) async-start(), calls=%async_computation.3 | async-start | bytes 6488064 | tf_op jit(solution)/shard_map/all_gather | solution.py:107
  34.3 280.8 %all-gather.8.cloned.1.call-start = ((), (), s32[]{:S(2)}) async-start(), calls=%async_computation.4 | async-start | bytes 6488064 | tf_op jit(solution)/shard_map/all_gather | solution.py:63
  34.9 94.1 %copy-start.4 = (f32[2048]{0:T(1024)S(1)}, f32[2048]{0:T(1024)}, u32[]{:S(2)}) copy-start(f32[2048]{0:T(1024)} %param.17) | copy-start | bytes 24580
  34.9 325.0 %reduce-scatter.2.cloned.1.call-start = ((), (), s32[]{:S(2)}) async-start(), calls=%async_computation.5 | async-start | bytes 2621440 | tf_op jit(solution)/shard_map/reduce_scatter | solution.py:112
Sparse Core Ops, SparseCore 0:
  33.2 53.7 all-reduce.1
  329.9 29.9 reduce-scatter.1
Sparse Core Ops, SparseCore 1:
  35.8 93.1 all-gather.3
  131.0 90.2 all-gather.5
  223.1 91.9 all-gather.7
where the time goes:
time: 371 us; the launch traced here: 370 us
  waiting for transfers between devices  302 us (81%)
  matrix products  29.3 us (8%)
  between operations  15.1 us (4%)
  other arithmetic  10.6 us (3%)
  local copies, waits for them, and re-layouts  6.13 us (2%)
  starting transfers between devices  5.4 us (1%)
    all_gather x1, waiting for transfers between devices, fetch_down(): return lax.all_gather(down_weight, 'sp', axis=1, tiled=True)  93.9 us
    all_gather x1, waiting for transfers between devices, shards(): up_sectioned = lax.all_gather(up_weight, 'sp', axis=0, tiled=True)  83.3 us
    psum x1, waiting for transfers between devices, shards(): lax.psum(jnp.dot(attended, out_weight, preferred_element_type=jnp.float32...  52.1 us
    all_gather x1, waiting for transfers between devices, shards(): gate_sectioned = lax.all_gather(gate_weight, 'sp', axis=0, tiled=True)  37 us
    reduce_scatter x1, waiting for transfers between devices, shards(): lax.psum_scatter(jnp.dot(hidden, down_whole, preferred_element_type=jnp.f...  30.2 us
    dot_general x1, matrix products, shards(): jnp.dot(hidden, down_whole, preferred_element_type=jnp.float32)  14.6 us
    dot_general x1, matrix products, shards(): jnp.dot(normed_all, gate_sectioned, preferred_element_type=jnp.float32)  8.96 us
  transfers between devices with their start and end apart: 7, of which 6 were waited for; matrix products, arithmetic and copies ran while one was open for 4% of the time, Pallas kernels for 0%

commit v1 on v0

--- a/solution.py
+++ b/solution.py
@@ -1,6 +1,10 @@
+import functools
+
 import jax
 import jax.numpy as jnp
 from jax import lax
+from jax.experimental import pallas as pl
+from jax.experimental.pallas import tpu as pltpu
 from jax.sharding import PartitionSpec as P
 
 DH = 128
@@ -117,6 +121,416 @@
     ).astype(jnp.float32)
     return (middle_own + ffn_share).astype(jnp.bfloat16)
 
+def ring_place(index, count):
+    row, side = index // 2, index % 2
+    return row * (1 - side) + (count - 1 - row) * side
+
+
+def ring_owner(place, count):
+    side = place // (count // 2)
+    row = place * (1 - side) + (count - 1 - place) * side
+    return 2 * row + side
+
+
+def layer_kernel(
+    q_ref, k_ref, v_ref, sink_ref, gain_ref, res_ref, ow_ref, g_ref, u_ref, d_ref, out_ref,
+    kx, vx, halo, ow, resid, attended, part, arecv, middle, nrm,
+    gbuf, ubuf, dbuf, gacc, uacc, hidden, fpart, frecv,
+    halo_s, halo_r, loc, ring_s, ring_r, attn_s, attn_r, nrm_s, nrm_r, ffn_s, ffn_r,
+    *, count, tps,
+):
+    me = lax.axis_index("sp")
+    mt = lax.axis_index("tp")
+    tok = q_ref.shape[0]
+    share = tok // tps
+    model = ow_ref.shape[1]
+    rows = g_ref.shape[0]
+    cols = d_ref.shape[1]
+    group = q_ref.shape[1] // k_ref.shape[1]
+    kv_heads = k_ref.shape[1] // DH
+    seq_len = tok * count
+    full = count // 2 - 1
+    opp = 2 * full
+    own = opp + 1
+    place = ring_place(me, count)
+    fore = ring_owner((place + 1) % count, count)
+    back = ring_owner((place + count - 1) % count, count)
+    after = (me + 1) % count
+    before = (me + count - 1) % count
+
+    barrier = pltpu.get_barrier_semaphore()
+    for target in (fore, back, after, before):
+        pl.semaphore_signal(
+            barrier, inc=1, device_id={"sp": target}, device_id_type=pl.DeviceIdType.MESH
+        )
+    for delta in range(1, tps):
+        pl.semaphore_signal(
+            barrier, inc=1, device_id={"tp": (mt + delta) % tps},
+            device_id_type=pl.DeviceIdType.MESH,
+        )
+    pl.semaphore_wait(barrier, 4 + tps - 1)
+
+    def remote(src, dst, send, recv, where):
+        return pltpu.make_async_remote_copy(
+            src_ref=src, dst_ref=dst, send_sem=send, recv_sem=recv,
+            device_id=where, device_id_type=pl.DeviceIdType.MESH,
+        )
+
+    halos = [
+        remote(k_ref.at[pl.ds(tok - WIN, WIN)], halo.at[0], halo_s.at[0], halo_r.at[0], {"sp": after}),
+        remote(v_ref.at[pl.ds(tok - WIN, WIN)], halo.at[1], halo_s.at[1], halo_r.at[1], {"sp": after}),
+        remote(k_ref.at[pl.ds(0, WIN)], halo.at[2], halo_s.at[2], halo_r.at[2], {"sp": before}),
+        remote(v_ref.at[pl.ds(0, WIN)], halo.at[3], halo_s.at[3], halo_r.at[3], {"sp": before}),
+    ]
+    for copy in halos:
+        copy.start()
+
+    originals = (g_ref, u_ref, d_ref)
+    stores = (gbuf, ubuf, dbuf)
+
+    def hop(kind, way, step):
+        store = stores[kind]
+        slot = lambda s: way * full + s - 1
+        sems = (ring_s.at[kind, way, step - 1], ring_r.at[kind, way, step - 1])
+        where = {"sp": (fore, back)[way]}
+        if step <= full:
+            src = originals[kind] if step == 1 else store.at[slot(step - 1)]
+            return remote(src, store.at[slot(step)], *sems, where)
+        half = store.shape[1] // 2
+        piece = pl.ds(way * half, half)
+        return remote(
+            store.at[slot(full), piece], store.at[opp, piece], *sems, where
+        )
+
+    def send(kind, step):
+        for way in range(2):
+            hop(kind, way, step).start()
+
+    def arrive(kind, step):
+        for way in range(2):
+            hop(kind, way, step).wait_recv()
+
+    for kind in range(3):
+        send(kind, 1)
+
+    locals_ = [
+        pltpu.make_async_copy(ow_ref, ow, loc.at[0]),
+        pltpu.make_async_copy(
+            res_ref.at[pl.ds(pl.multiple_of(mt * share, share), share)], resid, loc.at[1]
+        ),
+        pltpu.make_async_copy(g_ref, gbuf.at[own], loc.at[2]),
+        pltpu.make_async_copy(u_ref, ubuf.at[own], loc.at[3]),
+        pltpu.make_async_copy(d_ref, dbuf.at[own], loc.at[4]),
+    ]
+    for copy in locals_:
+        copy.start()
+
+    kx[pl.ds(WIN, tok)] = k_ref[...]
+    vx[pl.ds(WIN, tok)] = v_ref[...]
+    for copy in halos:
+        copy.wait_recv()
+    kx[pl.ds(0, WIN)] = halo[0]
+    vx[pl.ds(0, WIN)] = halo[1]
+    kx[pl.ds(WIN + tok, WIN)] = halo[2]
+    vx[pl.ds(WIN + tok, WIN)] = halo[3]
+    locals_[0].wait()
+
+    span = share + 2 * WIN
+    row_at = lax.broadcasted_iota(jnp.int32, (share, span), 0)
+    col_at = lax.broadcasted_iota(jnp.int32, (share, span), 1)
+
+    def attn_send(delta):
+        peer = (mt + delta) % tps
+        first = pl.multiple_of(peer * share, share)
+        return remote(
+            part.at[pl.ds(first, share)], arecv.at[delta - 1],
+            attn_s.at[delta - 1], attn_r.at[delta - 1], {"tp": peer},
+        )
+
+    def attend(delta, carry):
+        first = pl.multiple_of(((mt + delta) % tps) * share, share)
+        key_pos = me * tok + first - WIN + col_at
+        gap = col_at - row_at
+        allowed = (gap >= 0) & (gap <= 2 * WIN) & (key_pos >= 0) & (key_pos < seq_len)
+        for kv in range(kv_heads):
+            keys = kx[pl.ds(first, span), kv * DH:(kv + 1) * DH]
+            values = vx[pl.ds(first, span), kv * DH:(kv + 1) * DH]
+            for sub in range(group):
+                head = kv * group + sub
+                query = q_ref[pl.ds(first, share), head * DH:(head + 1) * DH]
+                scores = lax.dot_general(
+                    query, keys, (((1,), (1,)), ((), ())), preferred_element_type=jnp.float32
+                ) * DH ** (-0.5)
+                scores = jnp.where(allowed, scores, MASKED)
+                sink = sink_ref[head]
+                top = jnp.maximum(jnp.max(scores, axis=-1, keepdims=True), sink)
+                weights = jnp.exp(scores - top)
+                total = jnp.sum(weights, axis=-1, keepdims=True) + jnp.exp(sink - top)
+                prob = (weights / total).astype(jnp.bfloat16)
+                attended[:, head * DH:(head + 1) * DH] = jnp.dot(
+                    prob, values, preferred_element_type=jnp.float32
+                ).astype(jnp.bfloat16)
+        part[pl.ds(first, share)] = jnp.dot(
+            attended[...], ow[...], preferred_element_type=jnp.float32
+        ).astype(jnp.bfloat16)
+
+        @pl.when(delta < tps)
+        def _():
+            attn_send(delta).start()
+
+        return carry
+
+    lax.fori_loop(1, tps + 1, attend, 0)
+
+    arrive(0, 1)
+    send(0, 2)
+    arrive(1, 1)
+    send(1, 2)
+
+    mine = pl.ds(pl.multiple_of(mt * share, share), share)
+    locals_[1].wait()
+    for delta in range(1, tps):
+        attn_send(delta).wait_recv()
+    strip = 32
+
+    def norm_strip(index, carry):
+        at = pl.ds(pl.multiple_of(index * strip, strip), strip)
+        there = pl.ds(pl.multiple_of(mt * share + index * strip, strip), strip)
+        mid = resid[at].astype(jnp.float32) + part[there].astype(jnp.float32)
+        for slot in range(tps - 1):
+            mid = mid + arecv[slot, at].astype(jnp.float32)
+        middle[at] = mid
+        mean_square = jnp.mean(mid * mid, axis=-1, keepdims=True)
+        nrm[there] = (mid * lax.rsqrt(mean_square + EPSILON) * gain_ref[...]).astype(jnp.bfloat16)
+        return carry
+
+    lax.fori_loop(0, share // strip, norm_strip, 0)
+
+    def nrm_send(delta):
+        return remote(
+            nrm.at[mine], nrm.at[mine],
+            nrm_s.at[delta - 1], nrm_r.at[delta - 1], {"tp": (mt + delta) % tps},
+        )
+
+    def nrm_arrive(delta):
+        origin = (mt + tps - delta) % tps
+        there = pl.ds(pl.multiple_of(origin * share, share), share)
+        return remote(
+            nrm.at[there], nrm.at[there],
+            nrm_s.at[delta - 1], nrm_r.at[delta - 1], {"tp": (mt + delta) % tps},
+        )
+
+    for delta in range(1, tps):
+        nrm_send(delta).start()
+
+    arrive(2, 1)
+    send(2, 2)
+    arrive(0, 2)
+    send(0, 3)
+    for delta in range(1, tps):
+        nrm_arrive(delta).wait_recv()
+    for copy in locals_[2:]:
+        copy.wait()
+
+    band = tok // 2
+
+    def owner_of(slot):
+        if slot == own:
+            away = 0
+        elif slot == opp:
+            away = count // 2
+        elif slot < full:
+            away = count - slot - 1
+        else:
+            away = slot - full + 1
+        return ring_owner((place + away) % count, count)
+
+    def gate_up(slots, first):
+        def one(index, carry):
+            at = pl.ds(pl.multiple_of(index * band, band), band)
+            for acc, store in ((gacc, gbuf), (uacc, ubuf)):
+                total = None if first else acc[at]
+                for slot in slots:
+                    cut = pl.ds(pl.multiple_of(owner_of(slot) * rows, rows), rows)
+                    term = jnp.dot(
+                        nrm[at, cut], store[slot], preferred_element_type=jnp.float32
+                    )
+                    total = term if total is None else total + term
+                acc[at] = total
+            return carry
+
+        lax.fori_loop(0, tok // band, one, 0)
+
+    def pair(step):
+        return (step - 1, full + step - 1)
+
+    gate_up((own,), True)
+    gate_up(pair(1), False)
+    for step in range(2, full):
+        arrive(1, step)
+        send(1, step + 1)
+        gate_up(pair(step), False)
+        if step < full - 1:
+            arrive(2, step)
+            send(2, step + 1)
+        arrive(0, step + 1)
+        send(0, step + 2)
+    arrive(1, full)
+    send(1, full + 1)
+    arrive(2, full - 1)
+    send(2, full)
+    gate_up(pair(full), False)
+    arrive(0, full + 1)
+    arrive(1, full + 1)
+    gate_up((opp,), False)
+    half_rows = 64
+
+    def gated(index, carry):
+        at = pl.ds(pl.multiple_of(index * half_rows, half_rows), half_rows)
+        gate = gacc[at]
+        hidden[at] = (gate / (1.0 + jnp.exp(-gate)) * uacc[at]).astype(jnp.bfloat16)
+        return carry
+
+    lax.fori_loop(0, tok // half_rows, gated, 0)
+
+    def ffn_send(slot, delta):
+        peer = (mt + delta) % tps
+        first = pl.multiple_of(peer * share, share)
+        return remote(
+            fpart.at[slot, pl.ds(first, share)], frecv.at[slot, delta - 1],
+            ffn_s.at[slot, delta - 1], ffn_r.at[slot, delta - 1], {"tp": peer},
+        )
+
+    def down(slot):
+        def one(index, carry):
+            at = pl.ds(pl.multiple_of(index * band, band), band)
+            fpart[slot, at] = jnp.dot(
+                hidden[at], dbuf[slot], preferred_element_type=jnp.float32
+            ).astype(jnp.bfloat16)
+            return carry
+
+        lax.fori_loop(0, tok // band, one, 0)
+        for delta in range(1, tps):
+            ffn_send(slot, delta).start()
+
+    def finish(slot):
+        for delta in range(1, tps):
+            ffn_send(slot, delta).wait_recv()
+        cut = pl.ds(pl.multiple_of(owner_of(slot) * cols, cols), cols)
+        total = middle[:, cut] + fpart[slot, mine].astype(jnp.float32)
+        for other in range(tps - 1):
+            total = total + frecv[slot, other].astype(jnp.float32)
+        out_ref[:, cut] = total.astype(out_ref.dtype)
+
+    down(own)
+    for step in range(1, full):
+        for slot in pair(step):
+            down(slot)
+    arrive(2, full)
+    send(2, full + 1)
+    for slot in pair(full):
+        down(slot)
+    finish(own)
+    for step in range(1, full):
+        for slot in pair(step):
+            finish(slot)
+    arrive(2, full + 1)
+    down(opp)
+    for slot in pair(full):
+        finish(slot)
+    finish(opp)
+
+    for copy in halos:
+        copy.wait_send()
+    for kind in range(3):
+        for step in range(1, full + 2):
+            for way in range(2):
+                hop(kind, way, step).wait_send()
+    for delta in range(1, tps):
+        attn_send(delta).wait_send()
+        nrm_send(delta).wait_send()
+        for slot in range(count):
+            ffn_send(slot, delta).wait_send()
+
+
+def fused_shards(
+    queries, key_rows, value_rows, sink_logits, residual, norm_gain,
+    out_weight, gate_weight, up_weight, down_weight,
+):
+    count, tps = lax.axis_size("sp"), lax.axis_size("tp")
+    tok, model = residual.shape
+    share = tok // tps
+    rows, units = gate_weight.shape
+    cols = down_weight.shape[1]
+    full = count // 2 - 1
+    kv_cols = key_rows.shape[1]
+    bf, f32 = jnp.bfloat16, jnp.float32
+    vmem = pl.BlockSpec(memory_space=pltpu.VMEM)
+    away = pl.BlockSpec(memory_space=pl.ANY)
+    dma = pltpu.SemaphoreType.DMA
+    return pl.pallas_call(
+        functools.partial(layer_kernel, count=count, tps=tps),
+        out_shape=jax.ShapeDtypeStruct((share, model), bf),
+        in_specs=[vmem, vmem, vmem, pl.BlockSpec(memory_space=pltpu.SMEM), vmem]
+        + [away] * 5,
+        out_specs=vmem,
+        scratch_shapes=[
+            pltpu.VMEM((tok + 2 * WIN, kv_cols), bf),
+            pltpu.VMEM((tok + 2 * WIN, kv_cols), bf),
+            pltpu.VMEM((4, WIN, kv_cols), bf),
+            pltpu.VMEM(out_weight.shape, bf),
+            pltpu.VMEM((share, model), bf),
+            pltpu.VMEM((share, queries.shape[1]), bf),
+            pltpu.VMEM((tok, model), bf),
+            pltpu.VMEM((tps - 1, share, model), bf),
+            pltpu.VMEM((share, model), f32),
+            pltpu.VMEM((tok, model), bf),
+            pltpu.VMEM((count, rows, units), bf),
+            pltpu.VMEM((count, rows, units), bf),
+            pltpu.VMEM((count, units, cols), bf),
+            pltpu.VMEM((tok, units), f32),
+            pltpu.VMEM((tok, units), f32),
+            pltpu.VMEM((tok, units), bf),
+            pltpu.VMEM((count, tok, cols), bf),
+            pltpu.VMEM((count, tps - 1, share, cols), bf),
+            dma((4,)),
+            dma((4,)),
+            dma((5,)),
+            dma((3, 2, full + 1)),
+            dma((3, 2, full + 1)),
+            dma((tps - 1,)),
+            dma((tps - 1,)),
+            dma((tps - 1,)),
+            dma((tps - 1,)),
+            dma((count, tps - 1)),
+            dma((count, tps - 1)),
+        ],
+        compiler_params=pltpu.CompilerParams(
+            collective_id=0, has_side_effects=True, vmem_limit_bytes=60 * 1024 * 1024
+        ),
+    )(
+        queries, key_rows, value_rows, sink_logits, norm_gain.reshape(1, model),
+        residual, out_weight, gate_weight, up_weight, down_weight,
+    )
+
+
+def chosen(queries, key_rows, value_rows, sink_logits, residual, norm_gain,
+           out_weight, gate_weight, up_weight, down_weight):
+    count = lax.axis_size("sp")
+    share = queries.shape[0] // lax.axis_size("tp")
+    fits = (
+        count % 2 == 0
+        and 8 <= count <= 16
+        and share % 128 == 0
+        and gate_weight.shape[0] % 128 == 0
+        and gate_weight.shape[1] % 128 == 0
+        and down_weight.shape[1] % 128 == 0
+    )
+    return (fused_shards if fits else shards)(
+        queries, key_rows, value_rows, sink_logits, residual, norm_gain,
+        out_weight, gate_weight, up_weight, down_weight,
+    )
+
 
 def solution(mesh):
     placed = (
@@ -132,5 +546,5 @@
         P("tp", "sp"),
     )
     return jax.shard_map(
-        shards, mesh=mesh, in_specs=placed, out_specs=P(("sp", "tp"), None), check_vma=False
-    )
+        chosen, mesh=mesh, in_specs=placed, out_specs=P(("sp", "tp"), None), check_vma=False
+    )

time: 371 us -> 182 us (0.49)
  waiting for transfers between devices: 302 us -> 0 us
  Pallas kernels: 0 us -> 180 us
  matrix products: 29.3 us -> 0 us
  between operations: 15.1 us -> 0.01 us
  other arithmetic: 10.6 us -> 0 us
  starting transfers between devices: 5.4 us -> 0 us
  local copies, waits for them, and re-layouts: 6.13 us -> 1.88 us
    all_gather x3 -> x0, waiting for transfers between devices: 214 us -> none  [the longest x1 93.9 us: fetch_down(): return lax.all_gather(down_weight, 'sp', axis=1, tiled=True)]
    pallas_call x0 -> x1, Pallas kernels: none -> 180 us  [fused_shards(): pl.pallas_call(functools.partial(layer_kernel, count=count, tps=tps), out...]
    psum x1 -> x0, waiting for transfers between devices: 52.1 us -> none  [shards(): lax.psum(jnp.dot(attended, out_weight, preferred_element_type=jnp.float32...]
    reduce_scatter x1 -> x0, waiting for transfers between devices: 30.2 us -> none  [shards(): lax.psum_scatter(jnp.dot(hidden, down_whole, preferred_element_type=jnp.f...]
    dot_general x7 -> x0, matrix products: 29.3 us -> none  [the longest x1 14.6 us: shards(): jnp.dot(hidden, down_whole, preferred_element_type=jnp.float32)]
    ppermute x2 -> x0, starting transfers between devices: 5.23 us -> none  [the longest x1 3.94 us: with_halo(): lax.ppermute(tail, axis, [(i, (i + 1) % count) for i in range(ends)])]
    add x7 -> x0, other arithmetic: 5.04 us -> none  [the longest x1 4.86 us: shards(): middle_all = residual.astype(jnp.float32) + attn_full]
  transfers between devices with their start and end apart: 7 -> 0, of which waited for: 6 -> 0; matrix products, arithmetic and copies ran while one was open for 4% -> 0% of each run, Pallas kernels for 0% -> 0%
where the time goes in v1:
time: 182 us
  Pallas kernels  180 us (99%)
  local copies, waits for them, and re-layouts  1.88 us (1%)
    pallas_call x1, Pallas kernels, fused_shards(): pl.pallas_call(functools.partial(layer_kernel, count=count, tps=tps), out...  180 us

profile of v1, /device:TPU:1, one launch (start us, length us, event | category | flops | bytes accessed | tf_op | source)
XLA Modules:
  0.0 182.1 jit_solution(4586674348515363148)
XLA Ops:
  0.0 180.2 %shard_map.100 = bf16[128,2048]{1,0:T(8,128)(2,1)} custom-call(bf16[512,512]{1,0:T(8,128)(2,1)} %q_ref.1, bf16[512,128]{1,0:T(8,128)(2,1)} %k_ref.1, bf16[512,128]{1,0:T(8,128)(2,1)} %v_ref.1, f32[4]{0:T(128)} %sink_ref.1, f32[1,2048]{1,0:T(1,128)} %bitcast.1, bf16[512,2048]{1,0:T(8,128)(2,1)} %res_ref.1, bf16[512,2048]{1,0:T(8,128)(2,1)} %ow_ref.1, ...), custom_call_target="tpu_custom_call" | custom-call | tf_op jit(solution)/shard_map/pallas_call | solution.py:471
  180.2 1.9 %copy.12 = bf16[128,2048]{1,0:T(8,128)(2,1)} copy(bf16[128,2048]{1,0:T(8,128)(2,1)} %shard_map.100) | data formatting | bytes 1048576

commit v2 on v1

--- a/solution.py
+++ b/solution.py
@@ -121,22 +121,12 @@
     ).astype(jnp.float32)
     return (middle_own + ffn_share).astype(jnp.bfloat16)
 
-def ring_place(index, count):
-    row, side = index // 2, index % 2
-    return row * (1 - side) + (count - 1 - row) * side
-
-
-def ring_owner(place, count):
-    side = place // (count // 2)
-    row = place * (1 - side) + (count - 1 - place) * side
-    return 2 * row + side
-
-
 def layer_kernel(
     q_ref, k_ref, v_ref, sink_ref, gain_ref, res_ref, ow_ref, g_ref, u_ref, d_ref, out_ref,
-    kx, vx, halo, ow, resid, attended, part, arecv, middle, nrm,
+    kx, vx, halo, ow, resid, attended, part, arecv, middle, nown, nrm,
     gbuf, ubuf, dbuf, gacc, uacc, hidden, fpart, frecv,
-    halo_s, halo_r, loc, ring_s, ring_r, attn_s, attn_r, nrm_s, nrm_r, ffn_s, ffn_r,
+    halo_s, halo_r, loc, col_s, col_r, x_s, x_r, sib_s, sib_r,
+    attn_s, attn_r, nrm_s, nrm_r, fwd_s, ffn_s, ffn_r,
     *, count, tps,
 ):
     me = lax.axis_index("sp")
@@ -149,26 +139,29 @@
     group = q_ref.shape[1] // k_ref.shape[1]
     kv_heads = k_ref.shape[1] // DH
     seq_len = tok * count
-    full = count // 2 - 1
-    opp = 2 * full
-    own = opp + 1
-    place = ring_place(me, count)
-    fore = ring_owner((place + 1) % count, count)
-    back = ring_owner((place + count - 1) % count, count)
+    deep, wide = count // 2, tps // 2
+    z, x, y, c = me // 2, me % 2, mt // 2, mt % 2
+    p = z % 2
+    turn = 1 - 2 * (z // (deep // 2))
+    home_z = z - p + c
+    pair_z = z + 1 - 2 * p
     after = (me + 1) % count
     before = (me + count - 1) % count
 
+    def at_device(zz, xx, yy, cc):
+        return {"sp": 2 * zz + xx, "tp": 2 * yy + cc}
+
     barrier = pltpu.get_barrier_semaphore()
-    for target in (fore, back, after, before):
+    greeted = [{"sp": after}, {"sp": before}, {"sp": 2 * z + 1 - x}]
+    for dz in range(deep):
+        for dt in range(tps):
+            if dz or dt:
+                greeted.append({"sp": 2 * ((z + dz) % deep) + x, "tp": (mt + dt) % tps})
+    for target in greeted:
         pl.semaphore_signal(
-            barrier, inc=1, device_id={"sp": target}, device_id_type=pl.DeviceIdType.MESH
-        )
-    for delta in range(1, tps):
-        pl.semaphore_signal(
-            barrier, inc=1, device_id={"tp": (mt + delta) % tps},
-            device_id_type=pl.DeviceIdType.MESH,
-        )
-    pl.semaphore_wait(barrier, 4 + tps - 1)
+            barrier, inc=1, device_id=target, device_id_type=pl.DeviceIdType.MESH
+        )
+    pl.semaphore_wait(barrier, len(greeted))
 
     def remote(src, dst, send, recv, where):
         return pltpu.make_async_remote_copy(
@@ -188,42 +181,101 @@
     originals = (g_ref, u_ref, d_ref)
     stores = (gbuf, ubuf, dbuf)
 
-    def hop(kind, way, step):
-        store = stores[kind]
-        slot = lambda s: way * full + s - 1
-        sems = (ring_s.at[kind, way, step - 1], ring_r.at[kind, way, step - 1])
-        where = {"sp": (fore, back)[way]}
-        if step <= full:
-            src = originals[kind] if step == 1 else store.at[slot(step - 1)]
-            return remote(src, store.at[slot(step)], *sems, where)
-        half = store.shape[1] // 2
-        piece = pl.ds(way * half, half)
+    def piece(kind, owner, part_of):
+        half = stores[kind].shape[1] // 2
+        return stores[kind].at[owner, pl.ds(part_of * half, half)]
+
+    def column(kind, j, h):
+        half = stores[kind].shape[1] // 2
+        target = 2 * ((z // 2 + j) % (deep // 2)) + c
+        src = originals[kind].at[pl.ds(h * half, half)]
+        dst = piece(kind, me, h)
+        there = remote(
+            src, dst, col_s.at[kind, j, h], col_r.at[kind, z], at_device(target, x, y, h)
+        )
+        here = pltpu.make_async_copy(src, dst, col_r.at[kind, z])
+        return there, here, jnp.logical_and(c == p, c == h) if j == 0 else None
+
+    def start_either(there, here, stays):
+        if stays is None:
+            there.start()
+            return
+
+        @pl.when(stays)
+        def _():
+            here.start()
+
+        @pl.when(jnp.logical_not(stays))
+        def _():
+            there.start()
+
+    def end_either(there, stays):
+        if stays is None:
+            there.wait_send()
+            return
+
+        @pl.when(jnp.logical_not(stays))
+        def _():
+            there.wait_send()
+
+    for kind in range(3):
+        for j in range(deep // 2):
+            for h in range(2):
+                start_either(*column(kind, j, h))
+
+    def source_z(k):
+        return (z + k * turn + deep) % deep
+
+    def owner_of(k, side):
+        return 2 * source_z(k) + (x if side == 0 else 1 - x)
+
+    def across(kind, k):
+        zs = source_z(k)
+        own_piece = piece(kind, 2 * zs + x, c)
         return remote(
-            store.at[slot(full), piece], store.at[opp, piece], *sems, where
-        )
-
-    def send(kind, step):
-        for way in range(2):
-            hop(kind, way, step).start()
-
-    def arrive(kind, step):
-        for way in range(2):
-            hop(kind, way, step).wait_recv()
-
-    for kind in range(3):
-        send(kind, 1)
+            own_piece, own_piece, x_s.at[kind, k], x_r.at[kind, zs], at_device(z, 1 - x, y, c)
+        )
+
+    def across_in(kind, k):
+        zs = source_z(k)
+        own_piece = piece(kind, 2 * zs + 1 - x, c)
+        return remote(
+            own_piece, own_piece, x_s.at[kind, k], x_r.at[kind, zs], at_device(z, 1 - x, y, c)
+        )
+
+    def sibling(kind, side, k, part_of):
+        own_piece = piece(kind, owner_of(k, side), part_of)
+        return remote(
+            own_piece, own_piece, sib_s.at[kind, side, k], sib_r.at[kind, side, source_z(k)],
+            at_device(z, x, y, 1 - c),
+        )
+
+    def relay(kind, k):
+        zs = source_z(k)
+        own_piece = piece(kind, 2 * zs + x, c)
+        remote(
+            own_piece, own_piece, x_s.at[kind, k], col_r.at[kind, zs], at_device(z, 1 - x, y, c)
+        ).wait_recv()
+        across(kind, k).start()
+        sibling(kind, 0, k, c).start()
+
+    def relay_across(kind, k):
+        across_in(kind, k).wait_recv()
+        sibling(kind, 1, k, c).start()
+
+    def settle(kind, side, k):
+        sibling(kind, side, k, 1 - c).wait_recv()
 
     locals_ = [
         pltpu.make_async_copy(ow_ref, ow, loc.at[0]),
         pltpu.make_async_copy(
             res_ref.at[pl.ds(pl.multiple_of(mt * share, share), share)], resid, loc.at[1]
         ),
-        pltpu.make_async_copy(g_ref, gbuf.at[own], loc.at[2]),
-        pltpu.make_async_copy(u_ref, ubuf.at[own], loc.at[3]),
-        pltpu.make_async_copy(d_ref, dbuf.at[own], loc.at[4]),
     ]
     for copy in locals_:
         copy.start()
+    for kind in range(3):
+        relay(kind, 0)
 
     kx[pl.ds(WIN, tok)] = k_ref[...]
     vx[pl.ds(WIN, tok)] = v_ref[...]
@@ -282,10 +334,8 @@
 
     lax.fori_loop(1, tps + 1, attend, 0)
 
-    arrive(0, 1)
-    send(0, 2)
-    arrive(1, 1)
-    send(1, 2)
+    for k in range(1, deep):
+        relay(0, k)
 
     mine = pl.ds(pl.multiple_of(mt * share, share), share)
     locals_[1].wait()
@@ -301,49 +351,59 @@
             mid = mid + arecv[slot, at].astype(jnp.float32)
         middle[at] = mid
         mean_square = jnp.mean(mid * mid, axis=-1, keepdims=True)
-        nrm[there] = (mid * lax.rsqrt(mean_square + EPSILON) * gain_ref[...]).astype(jnp.bfloat16)
+        nown[at] = (mid * lax.rsqrt(mean_square + EPSILON) * gain_ref[...]).astype(jnp.bfloat16)
         return carry
 
     lax.fori_loop(0, share // strip, norm_strip, 0)
 
-    def nrm_send(delta):
+    def nrm_send(dy):
+        there = remote(
+            nown, nrm.at[mine], nrm_s.at[dy], nrm_r.at[mt], at_device(z, x, (y + dy) % wide, p)
+        )
+        here = pltpu.make_async_copy(nown, nrm.at[mine], nrm_r.at[mt])
+        return there, here, c == p if dy == 0 else None
+
+    def nrm_pair():
         return remote(
-            nrm.at[mine], nrm.at[mine],
-            nrm_s.at[delta - 1], nrm_r.at[delta - 1], {"tp": (mt + delta) % tps},
-        )
-
-    def nrm_arrive(delta):
-        origin = (mt + tps - delta) % tps
-        there = pl.ds(pl.multiple_of(origin * share, share), share)
+            nown, nrm.at[mine], nrm_s.at[wide], nrm_r.at[mt], at_device(pair_z, x, y, p)
+        )
+
+    def nrm_rows(dy, core):
+        origin = 2 * ((y + dy) % wide) + core
+        return origin, nrm.at[pl.ds(pl.multiple_of(origin * share, share), share)]
+
+    def nrm_wait(dy, core):
+        origin, block = nrm_rows(dy, core)
+        pltpu.make_async_copy(block, block, nrm_r.at[origin]).wait()
+
+    def nrm_forward(dy, core):
+        origin, block = nrm_rows(0, core)
         return remote(
-            nrm.at[there], nrm.at[there],
-            nrm_s.at[delta - 1], nrm_r.at[delta - 1], {"tp": (mt + delta) % tps},
-        )
-
-    for delta in range(1, tps):
-        nrm_send(delta).start()
-
-    arrive(2, 1)
-    send(2, 2)
-    arrive(0, 2)
-    send(0, 3)
-    for delta in range(1, tps):
-        nrm_arrive(delta).wait_recv()
-    for copy in locals_[2:]:
-        copy.wait()
+            block, block, fwd_s.at[dy - 1, core], nrm_r.at[origin],
+            at_device(z, x, (y + dy) % wide, c),
+        )
+
+    nrm_pair().start()
+    for dy in range(wide - 1, -1, -1):
+        start_either(*nrm_send(dy))
+    for k in range(deep):
+        relay_across(0, k)
+    for core in range(2):
+        nrm_wait(0, core)
+
+    @pl.when(c != p)
+    def _():
+        for dy in range(1, wide):
+            for core in range(2):
+                nrm_forward(dy, core).start()
+
+    for k in range(1, deep):
+        relay(1, k)
+    for dy in range(1, wide):
+        for core in range(2):
+            nrm_wait(dy, core)
 
     band = tok // 2
-
-    def owner_of(slot):
-        if slot == own:
-            away = 0
-        elif slot == opp:
-            away = count // 2
-        elif slot < full:
-            away = count - slot - 1
-        else:
-            away = slot - full + 1
-        return ring_owner((place + away) % count, count)
 
     def gate_up(slots, first):
         def one(index, carry):
@@ -351,7 +411,7 @@
             for acc, store in ((gacc, gbuf), (uacc, ubuf)):
                 total = None if first else acc[at]
                 for slot in slots:
-                    cut = pl.ds(pl.multiple_of(owner_of(slot) * rows, rows), rows)
+                    cut = pl.ds(pl.multiple_of(slot * rows, rows), rows)
                     term = jnp.dot(
                         nrm[at, cut], store[slot], preferred_element_type=jnp.float32
                     )
@@ -361,28 +421,25 @@
 
         lax.fori_loop(0, tok // band, one, 0)
 
-    def pair(step):
-        return (step - 1, full + step - 1)
-
-    gate_up((own,), True)
-    gate_up(pair(1), False)
-    for step in range(2, full):
-        arrive(1, step)
-        send(1, step + 1)
-        gate_up(pair(step), False)
-        if step < full - 1:
-            arrive(2, step)
-            send(2, step + 1)
-        arrive(0, step + 1)
-        send(0, step + 2)
-    arrive(1, full)
-    send(1, full + 1)
-    arrive(2, full - 1)
-    send(2, full)
-    gate_up(pair(full), False)
-    arrive(0, full + 1)
-    arrive(1, full + 1)
-    gate_up((opp,), False)
+    def pair(k):
+        return owner_of(k, 0), owner_of(k, 1)
+
+    def settle_pair(k):
+        for kind in range(2):
+            for side in range(2):
+                settle(kind, side, k)
+
+    for k in range(deep - 1):
+        relay_across(1, k)
+        settle_pair(k)
+        gate_up(pair(k), k == 0)
+    relay_across(1, deep - 1)
+    for k in range(1, deep):
+        relay(2, k)
+    settle_pair(deep - 1)
+    gate_up(pair(deep - 1), False)
+    half_rows = 64
+
     half_rows = 64
 
     def gated(index, carry):
@@ -395,11 +452,14 @@
 
     def ffn_send(slot, delta):
         peer = (mt + delta) % tps
-        first = pl.multiple_of(peer * share, share)
-        return remote(
-            fpart.at[slot, pl.ds(first, share)], frecv.at[slot, delta - 1],
-            ffn_s.at[slot, delta - 1], ffn_r.at[slot, delta - 1], {"tp": peer},
-        )
+        block = fpart.at[slot, pl.ds(pl.multiple_of(peer * share, share), share)]
+        spot = frecv.at[slot, 2 * y + p]
+        there = remote(
+            block, spot, ffn_s.at[slot, delta], ffn_r.at[slot, 2 * y + p],
+            {"sp": 2 * home_z + x, "tp": peer},
+        )
+        here = pltpu.make_async_copy(block, spot, ffn_r.at[slot, 2 * y + p])
+        return there, here, c == p if delta == 0 else None
 
     def down(slot):
         def one(index, carry):
@@ -410,47 +470,57 @@
             return carry
 
         lax.fori_loop(0, tok // band, one, 0)
-        for delta in range(1, tps):
-            ffn_send(slot, delta).start()
+        for delta in range(tps):
+            start_either(*ffn_send(slot, delta))
 
     def finish(slot):
-        for delta in range(1, tps):
-            ffn_send(slot, delta).wait_recv()
-        cut = pl.ds(pl.multiple_of(owner_of(slot) * cols, cols), cols)
-        total = middle[:, cut] + fpart[slot, mine].astype(jnp.float32)
-        for other in range(tps - 1):
+        cut = pl.ds(pl.multiple_of(slot * cols, cols), cols)
+        total = middle[:, cut]
+        for other in range(tps):
+            spot = frecv.at[slot, other]
+            pltpu.make_async_copy(spot, spot, ffn_r.at[slot, other]).wait()
             total = total + frecv[slot, other].astype(jnp.float32)
         out_ref[:, cut] = total.astype(out_ref.dtype)
 
-    down(own)
-    for step in range(1, full):
-        for slot in pair(step):
-            down(slot)
-    arrive(2, full)
-    send(2, full + 1)
-    for slot in pair(full):
-        down(slot)
-    finish(own)
-    for step in range(1, full):
-        for slot in pair(step):
-            finish(slot)
-    arrive(2, full + 1)
-    down(opp)
-    for slot in pair(full):
-        finish(slot)
-    finish(opp)
+    for k in range(deep):
+        settle(2, 0, k)
+        down(owner_of(k, 0))
+    for k in range(deep):
+        relay_across(2, k)
+        settle(2, 1, k)
+        down(owner_of(k, 1))
+    for side in range(2):
+        for k in range(deep):
+            finish(owner_of(k, side))
 
     for copy in halos:
         copy.wait_send()
     for kind in range(3):
-        for step in range(1, full + 2):
-            for way in range(2):
-                hop(kind, way, step).wait_send()
+        for j in range(deep // 2):
+            for h in range(2):
+                there, _, stays = column(kind, j, h)
+                end_either(there, stays)
+        for k in range(deep):
+            across(kind, k).wait_send()
+            for side in range(2):
+                sibling(kind, side, k, c).wait_send()
     for delta in range(1, tps):
         attn_send(delta).wait_send()
-        nrm_send(delta).wait_send()
-        for slot in range(count):
-            ffn_send(slot, delta).wait_send()
+    nrm_pair().wait_send()
+    for dy in range(wide):
+        there, _, stays = nrm_send(dy)
+        end_either(there, stays)
+
+    @pl.when(c != p)
+    def _():
+        for dy in range(1, wide):
+            for core in range(2):
+                nrm_forward(dy, core).wait_send()
+
+    for slot in range(count):
+        for delta in range(tps):
+            there, _, stays = ffn_send(slot, delta)
+            end_either(there, stays)
 
 
 def fused_shards(
@@ -462,7 +532,7 @@
     share = tok // tps
     rows, units = gate_weight.shape
     cols = down_weight.shape[1]
-    full = count // 2 - 1
+    deep, wide = count // 2, tps // 2
     kv_cols = key_rows.shape[1]
     bf, f32 = jnp.bfloat16, jnp.float32
     vmem = pl.BlockSpec(memory_space=pltpu.VMEM)
@@ -484,6 +554,7 @@
             pltpu.VMEM((tok, model), bf),
             pltpu.VMEM((tps - 1, share, model), bf),
             pltpu.VMEM((share, model), f32),
+            pltpu.VMEM((share, model), bf),
             pltpu.VMEM((tok, model), bf),
             pltpu.VMEM((count, rows, units), bf),
             pltpu.VMEM((count, rows, units), bf),
@@ -492,18 +563,23 @@
             pltpu.VMEM((tok, units), f32),
             pltpu.VMEM((tok, units), bf),
             pltpu.VMEM((count, tok, cols), bf),
-            pltpu.VMEM((count, tps - 1, share, cols), bf),
+            pltpu.VMEM((count, tps, share, cols), bf),
             dma((4,)),
             dma((4,)),
-            dma((5,)),
-            dma((3, 2, full + 1)),
-            dma((3, 2, full + 1)),
+            dma((2,)),
+            dma((3, deep // 2, 2)),
+            dma((3, deep)),
+            dma((3, deep)),
+            dma((3, deep)),
+            dma((3, 2, deep)),
+            dma((3, 2, deep)),
             dma((tps - 1,)),
             dma((tps - 1,)),
-            dma((tps - 1,)),
-            dma((tps - 1,)),
-            dma((count, tps - 1)),
-            dma((count, tps - 1)),
+            dma((wide + 1,)),
+            dma((tps,)),
+            dma((wide - 1, 2)),
+            dma((count, tps)),
+            dma((count, tps)),
         ],
         compiler_params=pltpu.CompilerParams(
             collective_id=0, has_side_effects=True, vmem_limit_bytes=60 * 1024 * 1024
@@ -519,8 +595,9 @@
     count = lax.axis_size("sp")
     share = queries.shape[0] // lax.axis_size("tp")
     fits = (
-        count % 2 == 0
+        count % 4 == 0
         and 8 <= count <= 16
+        and lax.axis_size("tp") == 4
         and share % 128 == 0
         and gate_weight.shape[0] % 128 == 0
         and gate_weight.shape[1] % 128 == 0

time: 182 us -> 152 us (0.84)
  Pallas kernels: 180 us -> 150 us
    pallas_call x1, Pallas kernels: 180 us -> 150 us  [fused_shards(): pl.pallas_call(functools.partial(layer_kernel, count=count, tps=tps), out...]
where the time goes in v2:
time: 152 us
  Pallas kernels  150 us (99%)
  local copies, waits for them, and re-layouts  1.88 us (1%)
    pallas_call x1, Pallas kernels, fused_shards(): pl.pallas_call(functools.partial(layer_kernel, count=count, tps=tps), out...  150 us

profile of v2, /device:TPU:1, one launch (start us, length us, event | category | flops | bytes accessed | tf_op | source)
XLA Modules:
  0.0 151.9 jit_solution(8336754571387351311)
XLA Ops:
  0.0 150.0 %shard_map.100 = bf16[128,2048]{1,0:T(8,128)(2,1)} custom-call(bf16[512,512]{1,0:T(8,128)(2,1)} %q_ref.1, bf16[512,128]{1,0:T(8,128)(2,1)} %k_ref.1, bf16[512,128]{1,0:T(8,128)(2,1)} %v_ref.1, f32[4]{0:T(128)} %sink_ref.1, f32[1,2048]{1,0:T(1,128)} %bitcast.1, bf16[512,2048]{1,0:T(8,128)(2,1)} %res_ref.1, bf16[512,2048]{1,0:T(8,128)(2,1)} %ow_ref.1, ...), custom_call_target="tpu_custom_call" | custom-call | tf_op jit(solution)/shard_map/pallas_call | solution.py:541
  150.0 1.9 %copy.12 = bf16[128,2048]{1,0:T(8,128)(2,1)} copy(bf16[128,2048]{1,0:T(8,128)(2,1)} %shard_map.100) | data formatting | bytes 1048576

commit v3 on v2

--- a/solution.py
+++ b/solution.py
@@ -218,10 +218,17 @@
         def _():
             there.wait_send()
 
-    for kind in range(3):
-        for j in range(deep // 2):
-            for h in range(2):
-                start_either(*column(kind, j, h))
+    def is_late(kind, j, h):
+        return kind == 2 or (kind == 1 and j > 0 and h == 1)
+
+    def columns(late):
+        for kind in range(3):
+            for j in range(deep // 2):
+                for h in range(2):
+                    if is_late(kind, j, h) == late:
+                        start_either(*column(kind, j, h))
+
+    columns(False)
 
     def source_z(k):
         return (z + k * turn + deep) % deep
@@ -274,7 +281,7 @@
     ]
     for copy in locals_:
         copy.start()
-    for kind in range(3):
+    for kind in range(2):
         relay(kind, 0)
 
     kx[pl.ds(WIN, tok)] = k_ref[...]
@@ -386,8 +393,12 @@
     nrm_pair().start()
     for dy in range(wide - 1, -1, -1):
         start_either(*nrm_send(dy))
+    columns(True)
     for k in range(deep):
         relay_across(0, k)
+    for k in range(1, deep):
+        relay(1, k)
+    relay(2, 0)
     for core in range(2):
         nrm_wait(0, core)
 
@@ -397,8 +408,6 @@
             for core in range(2):
                 nrm_forward(dy, core).start()
 
-    for k in range(1, deep):
-        relay(1, k)
     for dy in range(1, wide):
         for core in range(2):
             nrm_wait(dy, core)

time: 152 us -> 137 us (0.901)
  the two profiles are of different devices: /device:TPU:1 before, /device:TPU:24 now
where the time goes in v3:
time: 137 us
  Pallas kernels  135 us (99%)
  local copies, waits for them, and re-layouts  1.88 us (1%)
    pallas_call x1, Pallas kernels, fused_shards(): pl.pallas_call(functools.partial(layer_kernel, count=count, tps=tps), out...  135 us

profile of v3, /device:TPU:24, one launch (start us, length us, event | category | flops | bytes accessed | tf_op | source)
XLA Modules:
  0.0 137.2 jit_solution(9112480098943947112)
XLA Ops:
  0.0 135.3 %shard_map.100 = bf16[128,2048]{1,0:T(8,128)(2,1)} custom-call(bf16[512,512]{1,0:T(8,128)(2,1)} %q_ref.1, bf16[512,128]{1,0:T(8,128)(2,1)} %k_ref.1, bf16[512,128]{1,0:T(8,128)(2,1)} %v_ref.1, f32[4]{0:T(128)} %sink_ref.1, f32[1,2048]{1,0:T(1,128)} %bitcast.1, bf16[512,2048]{1,0:T(8,128)(2,1)} %res_ref.1, bf16[512,2048]{1,0:T(8,128)(2,1)} %ow_ref.1, ...), custom_call_target="tpu_custom_call" | custom-call | tf_op jit(solution)/shard_map/pallas_call | solution.py:550
  135.3 1.9 %copy.12 = bf16[128,2048]{1,0:T(8,128)(2,1)} copy(bf16[128,2048]{1,0:T(8,128)(2,1)} %shard_map.100) | data formatting | bytes 1048576
